TPU v7x, 32 devices: a whole 2x2x4 slice. The times are simulated.
32 devices in a mesh: sp: 8 (over z, y), tp: 4 (over x, core).
Axes of the slice: x: 2, y: 2, z: 4, core: 2. Of those that a mesh axis runs over, the one named last changes fastest.
Arguments:
- stream: bfloat16 [2048, 2048], P('sp', 'tp'), may hold values from -8 to 8
- norm_gain: float32 [2, 2048], P(None, 'tp'), may hold values from 0.1 to 1.9
- query_weight: bfloat16 [2, 2048, 1024], P(None, None, 'tp'), may hold values from -4 to 4
- key_weight: bfloat16 [2, 2048, 1024], P(None, None, 'tp'), may hold values from -4 to 4
- value_weight: bfloat16 [2, 2048, 1024], P(None, None, 'tp'), may hold values from -0.125 to 0.125
- out_weight: bfloat16 [2, 1024, 2048], P(None, None, 'tp'), may hold values from -1.5 to 1.5
- rel_bias: float32 [2, 16, 257], P(None, 'tp'), may hold values from -4 to 4
Outputs:
- mixed: bfloat16 [2048, 2048], P('sp', 'tp')
All inputs are finite; a program needn't handle non-finite values.
Results may differ from a plain program's by a relative error of at most 0.013.
Values may be sent and summed in bfloat16 or wider, within the bound.
A program may use at most 64 MiB of HBM per device.

v0:
```python
import jax
import jax.numpy as jnp
from jax import lax
from jax.sharding import PartitionSpec as P

D = 2048
SEG = 64
PREV = 8
CLIP = 128
LAYERS = 2
epsilon = 1e-06
masked_score = -1e30


def from_behind(shard, axis, by):
    count = lax.axis_size(axis)
    pairs = [(i, i + by) for i in range(count) if 0 <= i + by < count]
    return lax.ppermute(shard, axis, pairs)


def normalize(residual, gain):
    values_f = residual.astype(jnp.float32)
    squares = lax.psum(jnp.sum(values_f * values_f, axis=-1, keepdims=True), "tp")
    scaled = values_f * lax.rsqrt(squares / D + epsilon)
    return (scaled * gain).astype(jnp.bfloat16)


def bias_table(table, band_len):
    heads_here = table.shape[0]
    near_part = table[:, CLIP - (SEG - 1) :]
    far_count = band_len - 1 - CLIP
    far_part = jnp.broadcast_to(table[:, 2 * CLIP : 2 * CLIP + 1], (heads_here, far_count))
    reversed_row = jnp.concatenate([near_part, far_part], axis=1)[:, ::-1]
    slices = [
        reversed_row[:, SEG - 1 - within : SEG - 1 - within + band_len] for within in range(SEG)
    ]
    return jnp.stack(slices, axis=1)


def project_rows(rows_local, query_count, query_mat, key_mat, value_mat):
    row_count = rows_local.shape[0]
    first_query = row_count - query_count
    piece = lax.all_gather(rows_local, "tp", axis=1, tiled=True)
    query_sum = jnp.dot(piece[first_query:], query_mat, preferred_element_type=jnp.float32)
    key_sum = jnp.dot(piece, key_mat, preferred_element_type=jnp.float32)
    value_sum = jnp.dot(piece, value_mat, preferred_element_type=jnp.float32)
    return (
        query_sum.astype(jnp.bfloat16),
        key_sum.astype(jnp.bfloat16),
        value_sum.astype(jnp.bfloat16),
    )


def earlier_inputs(normed, shift_count):
    pieces = [from_behind(normed, "sp", step_back) for step_back in range(shift_count, 0, -1)]
    return jnp.concatenate(pieces, axis=0)


def band_blocks(extended, segments):
    blocked = extended.reshape((segments + PREV, SEG) + extended.shape[1:])
    return jnp.concatenate(
        [blocked[offset_seg : offset_seg + segments] for offset_seg in range(PREV + 1)], axis=1
    )


def attend(query_rows, key_ext, value_ext, position_bias, visible):
    tok_rows, head_cols = query_rows.shape
    heads_here = position_bias.shape[0]
    head_dim = head_cols // heads_here
    segments = tok_rows // SEG
    band_len = (PREV + 1) * SEG
    query_blocks = query_rows.reshape(segments, SEG, heads_here, head_dim)
    key_blocks = band_blocks(key_ext, segments).reshape(segments, band_len, heads_here, head_dim)
    value_blocks = band_blocks(value_ext, segments).reshape(
        segments, band_len, heads_here, head_dim
    )
    visible_blocks = band_blocks(visible, segments)
    scores = jnp.einsum(
        "sqhd,skhd->hsqk", query_blocks, key_blocks, preferred_element_type=jnp.float32
    )
    scores = scores * head_dim ** (-0.5) + position_bias[:, None]
    scores = jnp.where(visible_blocks[None, :, None, :], scores, masked_score)
    maximum = jnp.max(scores, axis=-1, keepdims=True)
    exponent = jnp.exp(scores - maximum)
    weights = (exponent / jnp.sum(exponent, axis=-1, keepdims=True)).astype(jnp.bfloat16)
    attended = jnp.einsum(
        "hsqk,skhd->sqhd", weights, value_blocks, preferred_element_type=jnp.float32
    )
    return attended.astype(jnp.bfloat16).reshape(tok_rows, head_cols)


def per_device(stream, norm_gain, query_weight, key_weight, value_weight, out_weight, rel_bias):
    tok_rows = stream.shape[0]
    reach_rows = PREV * SEG
    shift_count = max(1, reach_rows // tok_rows)
    band_len = reach_rows + SEG
    positions = (
        lax.axis_index("sp") * tok_rows
        - reach_rows
        + jnp.arange(reach_rows + tok_rows, dtype=jnp.int32)
    )
    visible = positions >= 0
    residual = stream
    for layer_index in range(LAYERS):
        normed = normalize(residual, norm_gain[layer_index])
        normed_ext = jnp.concatenate([earlier_inputs(normed, shift_count), normed], axis=0)
        query_rows, key_ext, value_ext = project_rows(
            normed_ext,
            tok_rows,
            query_weight[layer_index],
            key_weight[layer_index],
            value_weight[layer_index],
        )
        position_bias = bias_table(rel_bias[layer_index], band_len)
        attended = attend(query_rows, key_ext, value_ext, position_bias, visible)
        out_mat = out_weight[layer_index]
        summed = residual.astype(jnp.float32) + jnp.dot(
            lax.all_gather(attended, "tp", axis=1, tiled=True),
            out_mat,
            preferred_element_type=jnp.float32,
        )
        residual = summed.astype(jnp.bfloat16)
    return residual


def solution(mesh):
    placed = (
        P("sp", "tp"),
        P(None, "tp"),
        P(None, None, "tp"),
        P(None, None, "tp"),
        P(None, None, "tp"),
        P(None, None, "tp"),
        P(None, "tp", None),
    )
    return jax.shard_map(
        per_device, mesh=mesh, in_specs=placed, out_specs=P("sp", "tp"), check_vma=False
    )
```

profile of v0, /device:TPU:0, one launch (start us, length us, event | category | flops | bytes accessed | tf_op | source)
XLA Modules:
  0.0 262.6 jit_solution(17611809908315193769)
XLA Ops:
  6.5 1.1 fusion.49
  7.6 8.4 %psum.14 = f32[256,1]{0,1:T(1,128)S(1)} all-reduce(f32[256,1]{0,1:T(1,128)S(1)} %bitcast.562), channel_id=1, replica_groups=mesh['sp'=8,'tp'=4] {'tp'}, use_global_device_ids=true, to_apply=%region_1.0 | all-reduce | flops 256 | bytes 2048 | tf_op jit(solution)/shard_map/psum | solution.py:23
  16.8 1.1 fusion.51
  17.9 3.4 %collective-permute-start.1 = (bf16[256,512]{1,0:T(8,128)(2,1)S(1)}, bf16[256,512]{1,0:T(8,128)(2,1)S(1)}, u32[]{:S(2)}, u32[]{:S(2)}) collective-permute-start(bf16[256,512]{1,0:T(8,128)(2,1)S(1)} %fusion.51), channel_id=1, source_target_pairs={{0,4},{4,8},{8,12},{12,16},{16,20},{20,24},{24,28},{1,5},{5,9},{9,... | collective-permute-start | bytes 786440 | tf_op jit(solution)/shard_map/ppermute | solution.py:18
  21.3 3.5 %collective-permute-start = (bf16[256,512]{1,0:T(8,128)(2,1)S(1)}, bf16[256,512]{1,0:T(8,128)(2,1)S(1)}, u32[]{:S(2)}, u32[]{:S(2)}) collective-permute-start(bf16[256,512]{1,0:T(8,128)(2,1)S(1)} %fusion.51), channel_id=1, source_target_pairs={{0,8},{4,12},{8,16},{12,20},{16,24},{20,28},{1,9},{5,13},{9,17},{1... | collective-permute-start | bytes 786440 | tf_op jit(solution)/shard_map/ppermute | solution.py:18
  87.8 0.9 pad_maximum_fusion
  95.7 2.0 reverse.211
  98.3 6.1 %stack.454 = f32[4,64,576]{2,1,0:T(8,128)} concatenate(f32[4,1,576]{2,1,0:T(1,128)S(1)} %copy.193, f32[4,1,576]{2,1,0:T(1,128)S(1)} %copy.194, f32[4,1,576]{2,1,0:T(1,128)S(1)} %copy.195, f32[4,1,576]{2,1,0:T(1,128)S(1)} %copy.196, f32[4,1,576]{2,1,0:T(1,128)S(1)} %copy.197, f32[4,1,576]{2,1,0:T(1,128)S(1)} %copy.198, f32[4,1,576]{2,1,0:T(1,128)S(1)} %copy.199, ...), dimensions={1} | concatenate | bytes 1179648 | tf_op jit(solution)/shard_map/stack | solution.py:37
  118.5 2.1 convolution_convert_fusion.5
  121.5 2.2 convolution_convert_fusion.3
  127.8 3.1 %convolution_convert_fusion.2 = bf16[768,256]{1,0:T(8,128)(2,1)S(1)} fusion(bf16[768,2048]{1,0:T(8,128)(2,1)} %all-gather.3.cloned.1.call-done, bf16[2,2048,256]{2,1,0:T(8,128)(2,1)} %param.10), kind=kOutput, calls=%fused_computation.24 | convolution fusion | flops 805502976 | bytes 4587520 | tf_op jit(solution)/shard_map/dot_general | solution.py:45
  131.3 0.9 copy.191
  132.3 0.9 copy.190
  133.4 0.9 copy.189
  134.5 0.9 copy.188
  135.6 0.9 copy.187
  136.7 0.9 copy.186
  137.7 0.9 copy.185
  138.8 0.9 copy.184
  140.8 2.8 %concatenate.125 = bf16[4,576,4,64]{1,3,0,2:T(8,128)(2,1)S(1)} concatenate(bf16[4,64,4,64]{1,3,0,2:T(8,128)(2,1)} %copy.183, bf16[4,64,4,64]{1,3,0,2:T(8,128)(2,1)} %copy.184, bf16[4,64,4,64]{1,3,0,2:T(8,128)(2,1)} %copy.185, bf16[4,64,4,64]{1,3,0,2:T(8,128)(2,1)} %copy.186, bf16[4,64,4,64]{1,3,0,2:T(8,128)(2,1)} %copy.187, bf16[4,64,4,64]{1,3,0,2:T(8,128)(2,1)} %copy.188, ...), dimensions={1} | concatenate | bytes 2359296 | tf_op jit(solution)/shard_map/concatenate | solution.py:61
  143.6 3.7 %fusion.204 = (f32[4,4,64]{2,1,0:T(4,128)S(1)}, f32[4,4,64,576]{3,2,1,0:T(8,128)}) fusion(f32[4,64,576]{2,1,0:T(8,128)} %stack.454, pred[4,576]{1,0:T(4,128)(4,1)S(1)} %copy-done.42, bf16[4,576,4,64]{1,3,0,2:T(8,128)(2,1)S(1)} %concatenate.125, bf16[4,64,4,64]{3,2,1,0:T(4,128)(2,1)} %reshape.164), kind=kOutput, calls=%fused_computation.465 | convolution fusion | flops 78447168 | bytes 4266240 | tf_op jit(solution)/shard_map/sub | solution.py:84
  147.3 2.3 concatenate.114
  149.6 2.4 fusion.28
  152.6 6.6 %all_gather.13 = bf16[256,1024]{1,0:T(8,128)(2,1)S(1)} all-gather(bf16[256,256]{1,0:T(8,128)(2,1)S(1)} %reshape.165), channel_id=1, replica_groups=mesh['sp'=8,'tp'=4] {'tp'}, dimensions={1}, use_global_device_ids=true | all-gather | bytes 655360 | tf_op jit(solution)/shard_map/all_gather | solution.py:118
  159.5 1.8 multiply_reduce_fusion
  161.3 6.8 %psum.15 = f32[256,1]{0,1:T(1,128)S(1)} all-reduce(f32[256,1]{0,1:T(1,128)S(1)} %bitcast.563), channel_id=1, replica_groups=mesh['sp'=8,'tp'=4] {'tp'}, use_global_device_ids=true, to_apply=%region_5.6 | all-reduce | flops 256 | bytes 2048 | tf_op jit(solution)/shard_map/psum | solution.py:23
  168.2 3.4 %collective-permute-start.3 = (bf16[256,512]{1,0:T(8,128)(2,1)S(1)}, bf16[256,512]{1,0:T(8,128)(2,1)S(1)}, u32[]{:S(2)}, u32[]{:S(2)}) collective-permute-start(bf16[256,512]{1,0:T(8,128)(2,1)S(1)} %multiply_convert_fusion), channel_id=1, source_target_pairs={{0,4},{4,8},{8,12},{12,16},{16,20},{20,24},{24,28},{1,5},{5,9},{9,... | collective-permute-start | bytes 786440 | tf_op jit(solution)/shard_map/ppermute | solution.py:18
  171.7 3.5 %collective-permute-start.2 = (bf16[256,512]{1,0:T(8,128)(2,1)S(1)}, bf16[256,512]{1,0:T(8,128)(2,1)S(1)}, u32[]{:S(2)}, u32[]{:S(2)}) collective-permute-start(bf16[256,512]{1,0:T(8,128)(2,1)S(1)} %multiply_convert_fusion), channel_id=1, source_target_pairs={{0,8},{4,12},{8,16},{12,20},{16,24},{20,28},{1,9},{5,13},{9,17},{1... | collective-permute-start | bytes 786440 | tf_op jit(solution)/shard_map/ppermute | solution.py:18
  182.6 0.9 pad_maximum_fusion.1
  195.0 6.1 %stack.519 = f32[4,64,576]{2,1,0:T(8,128)} concatenate(f32[4,1,576]{2,1,0:T(1,128)S(1)} %copy.277, f32[4,1,576]{2,1,0:T(1,128)S(1)} %copy.278, f32[4,1,576]{2,1,0:T(1,128)S(1)} %copy.279, f32[4,1,576]{2,1,0:T(1,128)S(1)} %copy.280, f32[4,1,576]{2,1,0:T(1,128)S(1)} %copy.281, f32[4,1,576]{2,1,0:T(1,128)S(1)} %copy.282, f32[4,1,576]{2,1,0:T(1,128)S(1)} %copy.283, ...), dimensions={1} | concatenate | bytes 1179648 | tf_op jit(solution)/shard_map/stack | solution.py:37
  201.1 11.2 %all-gather.5.cloned.1.call-done = bf16[768,2048]{1,0:T(8,128)(2,1)} async-done(((bf16[768,512]{1,0:T(8,128)(2,1)}), bf16[768,2048]{1,0:T(8,128)(2,1)}) %all-gather.5.cloned.1.call-update) | async-done | bytes 3145744 | tf_op jit(solution)/shard_map/all_gather | solution.py:43
  212.2 2.1 convolution_convert_fusion.4
  215.3 2.2 convolution_convert_fusion.1
  221.6 3.2 %convolution_convert_fusion = bf16[768,256]{1,0:T(8,128)(2,1)S(1)} fusion(bf16[768,2048]{1,0:T(8,128)(2,1)} %all-gather.5.cloned.1.call-done, bf16[2,2048,256]{2,1,0:T(8,128)(2,1)} %param.10), kind=kOutput, calls=%fused_computation.22 | convolution fusion | flops 805502976 | bytes 4587520 | tf_op jit(solution)/shard_map/dot_general | solution.py:45
  225.0 0.9 copy.275
  226.1 0.9 copy.274
  227.2 0.9 copy.273
  228.3 0.9 copy.272
  229.3 0.9 copy.271
  230.4 0.9 copy.270
  231.5 0.9 copy.269
  232.6 0.9 copy.268
  234.6 2.8 %concatenate.147 = bf16[4,576,4,64]{1,3,0,2:T(8,128)(2,1)S(1)} concatenate(bf16[4,64,4,64]{1,3,0,2:T(8,128)(2,1)} %copy.267, bf16[4,64,4,64]{1,3,0,2:T(8,128)(2,1)} %copy.268, bf16[4,64,4,64]{1,3,0,2:T(8,128)(2,1)} %copy.269, bf16[4,64,4,64]{1,3,0,2:T(8,128)(2,1)} %copy.270, bf16[4,64,4,64]{1,3,0,2:T(8,128)(2,1)} %copy.271, bf16[4,64,4,64]{1,3,0,2:T(8,128)(2,1)} %copy.272, ...), dimensions={1} | concatenate | bytes 2359296 | tf_op jit(solution)/shard_map/concatenate | solution.py:61
  237.4 3.7 %fusion.207 = (f32[4,4,64]{2,1,0:T(4,128)S(1)}, f32[4,4,64,576]{3,2,1,0:T(8,128)}) fusion(f32[4,64,576]{2,1,0:T(8,128)} %stack.519, pred[4,576]{1,0:T(4,128)(4,1)S(1)} %copy-done.43, bf16[4,576,4,64]{1,3,0,2:T(8,128)(2,1)S(1)} %concatenate.147, bf16[4,64,4,64]{3,2,1,0:T(4,128)(2,1)} %reshape.166), kind=kOutput, calls=%fused_computation.466 | convolution fusion | flops 78447168 | bytes 4266240 | tf_op jit(solution)/shard_map/sub | solution.py:84
  241.1 2.3 concatenate.137
  243.4 2.4 fusion.25
  246.2 7.2 %all_gather.15 = bf16[256,1024]{1,0:T(8,128)(2,1)S(1)} all-gather(bf16[256,256]{1,0:T(8,128)(2,1)S(1)} %reshape.167), channel_id=1, replica_groups=mesh['sp'=8,'tp'=4] {'tp'}, dimensions={1}, use_global_device_ids=true | all-gather | bytes 655360 | tf_op jit(solution)/shard_map/all_gather | solution.py:118
  253.4 2.4 fusion.17
  (579 shorter events, 118.6 us)
Async XLA Ops:
  6.5 112.0 %all-gather.3.cloned.1.call-start = ((), (), s32[]{:S(2)}) async-start(), calls=%async_computation | async-start | bytes 3932160 | tf_op jit(solution)/shard_map/all_gather | solution.py:43
  17.9 70.0 %collective-permute-start.1 = (bf16[256,512]{1,0:T(8,128)(2,1)S(1)}, bf16[256,512]{1,0:T(8,128)(2,1)S(1)}, u32[]{:S(2)}, u32[]{:S(2)}) collective-permute-start(bf16[256,512]{1,0:T(8,128)(2,1)S(1)} %fusion.51), channel_id=1, source_target_pairs={{0,4},{4,8},{8,12},{12,16},{16,20},{20,24},{24,28},{1,5},{5,9},{9,... | collective-permute-start | bytes 786440 | tf_op jit(solution)/shard_map/ppermute | solution.py:18
  21.3 66.5 %collective-permute-start = (bf16[256,512]{1,0:T(8,128)(2,1)S(1)}, bf16[256,512]{1,0:T(8,128)(2,1)S(1)}, u32[]{:S(2)}, u32[]{:S(2)}) collective-permute-start(bf16[256,512]{1,0:T(8,128)(2,1)S(1)} %fusion.51), channel_id=1, source_target_pairs={{0,8},{4,12},{8,16},{12,20},{16,24},{20,28},{1,9},{5,13},{9,17},{1... | collective-permute-start | bytes 786440 | tf_op jit(solution)/shard_map/ppermute | solution.py:18
  88.8 123.4 %all-gather.5.cloned.1.call-start = ((), (), s32[]{:S(2)}) async-start(), calls=%async_computation.1 | async-start | bytes 3932160 | tf_op jit(solution)/shard_map/all_gather | solution.py:43
  149.6 9.7 %copy-start = (bf16[256,512]{1,0:T(8,128)(2,1)S(1)}, bf16[256,512]{1,0:T(8,128)(2,1)}, u32[]{:S(2)}) copy-start(bf16[256,512]{1,0:T(8,128)(2,1)} %param.7) | copy-start | bytes 786436
  152.5 22.7 %copy-start.27 = (f32[4,640]{1,0:T(4,128)S(1)}, f32[4,640]{1,0:T(4,128)}, u32[]{:S(2)}) copy-start(f32[4,640]{1,0:T(4,128)} %reverse.211) | copy-start | bytes 30724
  152.5 22.8 %copy-start.7 = (f32[4,1,576]{2,0,1:T(4,128)S(1)}, f32[4,1,576]{2,0,1:T(4,128)}, u32[]{:S(2)}) copy-start(f32[4,1,576]{2,0,1:T(4,128)} %slice_bitcast_fusion.8) | copy-start | bytes 27652
  152.5 22.8 %copy-start.8 = (f32[4,1,576]{2,0,1:T(4,128)S(1)}, f32[4,1,576]{2,0,1:T(4,128)}, u32[]{:S(2)}) copy-start(f32[4,1,576]{2,0,1:T(4,128)} %slice_bitcast_fusion.7) | copy-start | bytes 27652
  152.5 22.8 %copy-start.9 = (f32[4,1,576]{2,0,1:T(4,128)S(1)}, f32[4,1,576]{2,0,1:T(4,128)}, u32[]{:S(2)}) copy-start(f32[4,1,576]{2,0,1:T(4,128)} %slice_bitcast_fusion.16) | copy-start | bytes 27652
  152.5 22.8 %copy-start.10 = (f32[4,1,576]{2,0,1:T(4,128)S(1)}, f32[4,1,576]{2,0,1:T(4,128)}, u32[]{:S(2)}) copy-start(f32[4,1,576]{2,0,1:T(4,128)} %slice_bitcast_fusion.15) | copy-start | bytes 27652
  152.5 22.9 %copy-start.11 = (f32[4,1,576]{2,0,1:T(4,128)S(1)}, f32[4,1,576]{2,0,1:T(4,128)}, u32[]{:S(2)}) copy-start(f32[4,1,576]{2,0,1:T(4,128)} %slice_bitcast_fusion.14) | copy-start | bytes 27652
  152.5 22.9 %copy-start.12 = (f32[4,1,576]{2,0,1:T(4,128)S(1)}, f32[4,1,576]{2,0,1:T(4,128)}, u32[]{:S(2)}) copy-start(f32[4,1,576]{2,0,1:T(4,128)} %slice_bitcast_fusion.13) | copy-start | bytes 27652
  152.5 22.9 %copy-start.13 = (f32[4,1,576]{2,0,1:T(4,128)S(1)}, f32[4,1,576]{2,0,1:T(4,128)}, u32[]{:S(2)}) copy-start(f32[4,1,576]{2,0,1:T(4,128)} %slice_bitcast_fusion.12) | copy-start | bytes 27652
  152.5 22.9 %copy-start.14 = (f32[4,1,576]{2,0,1:T(4,128)S(1)}, f32[4,1,576]{2,0,1:T(4,128)}, u32[]{:S(2)}) copy-start(f32[4,1,576]{2,0,1:T(4,128)} %slice_bitcast_fusion.11) | copy-start | bytes 27652
  152.6 22.9 %copy-start.15 = (f32[4,1,576]{2,0,1:T(4,128)S(1)}, f32[4,1,576]{2,0,1:T(4,128)}, u32[]{:S(2)}) copy-start(f32[4,1,576]{2,0,1:T(4,128)} %slice_bitcast_fusion.10) | copy-start | bytes 27652
  152.6 23.0 %copy-start.16 = (f32[4,1,576]{2,0,1:T(4,128)S(1)}, f32[4,1,576]{2,0,1:T(4,128)}, u32[]{:S(2)}) copy-start(f32[4,1,576]{2,0,1:T(4,128)} %slice_bitcast_fusion.9) | copy-start | bytes 27652
  152.6 23.0 %copy-start.17 = (f32[4,1,576]{2,0,1:T(4,128)S(1)}, f32[4,1,576]{2,0,1:T(4,128)}, u32[]{:S(2)}) copy-start(f32[4,1,576]{2,0,1:T(4,128)} %slice_bitcast_fusion.6) | copy-start | bytes 27652
  152.6 23.0 %copy-start.18 = (f32[4,1,576]{2,0,1:T(4,128)S(1)}, f32[4,1,576]{2,0,1:T(4,128)}, u32[]{:S(2)}) copy-start(f32[4,1,576]{2,0,1:T(4,128)} %slice_bitcast_fusion.24) | copy-start | bytes 27652
  152.6 23.0 %copy-start.19 = (f32[4,1,576]{2,0,1:T(4,128)S(1)}, f32[4,1,576]{2,0,1:T(4,128)}, u32[]{:S(2)}) copy-start(f32[4,1,576]{2,0,1:T(4,128)} %slice_bitcast_fusion.23) | copy-start | bytes 27652
  152.6 23.0 %copy-start.20 = (f32[4,1,576]{2,0,1:T(4,128)S(1)}, f32[4,1,576]{2,0,1:T(4,128)}, u32[]{:S(2)}) copy-start(f32[4,1,576]{2,0,1:T(4,128)} %slice_bitcast_fusion.22) | copy-start | bytes 27652
  152.6 23.1 %copy-start.21 = (f32[4,1,576]{2,0,1:T(4,128)S(1)}, f32[4,1,576]{2,0,1:T(4,128)}, u32[]{:S(2)}) copy-start(f32[4,1,576]{2,0,1:T(4,128)} %slice_bitcast_fusion.21) | copy-start | bytes 27652
  152.6 23.1 %copy-start.22 = (f32[4,1,576]{2,0,1:T(4,128)S(1)}, f32[4,1,576]{2,0,1:T(4,128)}, u32[]{:S(2)}) copy-start(f32[4,1,576]{2,0,1:T(4,128)} %slice_bitcast_fusion.20) | copy-start | bytes 27652
  159.3 16.5 %copy-start.23 = (f32[4,1,576]{2,0,1:T(4,128)S(1)}, f32[4,1,576]{2,0,1:T(4,128)}, u32[]{:S(2)}) copy-start(f32[4,1,576]{2,0,1:T(4,128)} %slice_bitcast_fusion.19) | copy-start | bytes 27652
  159.3 16.5 %copy-start.24 = (f32[4,1,576]{2,0,1:T(4,128)S(1)}, f32[4,1,576]{2,0,1:T(4,128)}, u32[]{:S(2)}) copy-start(f32[4,1,576]{2,0,1:T(4,128)} %slice_bitcast_fusion.18) | copy-start | bytes 27652
  159.3 16.5 %copy-start.25 = (f32[4,1,576]{2,0,1:T(4,128)S(1)}, f32[4,1,576]{2,0,1:T(4,128)}, u32[]{:S(2)}) copy-start(f32[4,1,576]{2,0,1:T(4,128)} %slice_bitcast_fusion.17) | copy-start | bytes 27652
  159.3 16.5 %copy-start.26 = (f32[4,1,576]{2,0,1:T(4,128)S(1)}, f32[4,1,576]{2,0,1:T(4,128)}, u32[]{:S(2)}) copy-start(f32[4,1,576]{2,0,1:T(4,128)} %slice_bitcast_fusion.5) | copy-start | bytes 27652
  159.3 16.6 %copy-start.28 = (f32[4,1,576]{2,0,1:T(4,128)S(1)}, f32[4,1,576]{2,0,1:T(4,128)}, u32[]{:S(2)}) copy-start(f32[4,1,576]{2,0,1:T(4,128)} %slice_bitcast_fusion.32) | copy-start | bytes 27652
  159.3 16.6 %copy-start.29 = (f32[4,1,576]{2,0,1:T(4,128)S(1)}, f32[4,1,576]{2,0,1:T(4,128)}, u32[]{:S(2)}) copy-start(f32[4,1,576]{2,0,1:T(4,128)} %slice_bitcast_fusion.31) | copy-start | bytes 27652
  159.3 16.6 %copy-start.30 = (f32[4,1,576]{2,0,1:T(4,128)S(1)}, f32[4,1,576]{2,0,1:T(4,128)}, u32[]{:S(2)}) copy-start(f32[4,1,576]{2,0,1:T(4,128)} %slice_bitcast_fusion.30) | copy-start | bytes 27652
  159.3 16.6 %copy-start.31 = (f32[4,1,576]{2,0,1:T(4,128)S(1)}, f32[4,1,576]{2,0,1:T(4,128)}, u32[]{:S(2)}) copy-start(f32[4,1,576]{2,0,1:T(4,128)} %slice_bitcast_fusion.29) | copy-start | bytes 27652
  159.3 16.6 %copy-start.32 = (f32[4,1,576]{2,0,1:T(4,128)S(1)}, f32[4,1,576]{2,0,1:T(4,128)}, u32[]{:S(2)}) copy-start(f32[4,1,576]{2,0,1:T(4,128)} %slice_bitcast_fusion.28) | copy-start | bytes 27652
  159.3 16.7 %copy-start.33 = (f32[4,1,576]{2,0,1:T(4,128)S(1)}, f32[4,1,576]{2,0,1:T(4,128)}, u32[]{:S(2)}) copy-start(f32[4,1,576]{2,0,1:T(4,128)} %slice_bitcast_fusion.27) | copy-start | bytes 27652
  159.4 16.7 %copy-start.34 = (f32[4,1,576]{2,0,1:T(4,128)S(1)}, f32[4,1,576]{2,0,1:T(4,128)}, u32[]{:S(2)}) copy-start(f32[4,1,576]{2,0,1:T(4,128)} %slice_bitcast_fusion.26) | copy-start | bytes 27652
  159.4 16.7 %copy-start.35 = (f32[4,1,576]{2,0,1:T(4,128)S(1)}, f32[4,1,576]{2,0,1:T(4,128)}, u32[]{:S(2)}) copy-start(f32[4,1,576]{2,0,1:T(4,128)} %slice_bitcast_fusion.25) | copy-start | bytes 27652
  159.4 16.7 %copy-start.36 = (f32[4,1,576]{2,0,1:T(4,128)S(1)}, f32[4,1,576]{2,0,1:T(4,128)}, u32[]{:S(2)}) copy-start(f32[4,1,576]{2,0,1:T(4,128)} %slice_bitcast_fusion.4) | copy-start | bytes 27652
  159.4 16.7 %copy-start.37 = (f32[4,1,576]{2,0,1:T(4,128)S(1)}, f32[4,1,576]{2,0,1:T(4,128)}, u32[]{:S(2)}) copy-start(f32[4,1,576]{2,0,1:T(4,128)} %slice_bitcast_fusion.40) | copy-start | bytes 27652
  159.4 16.8 %copy-start.38 = (f32[4,1,576]{2,0,1:T(4,128)S(1)}, f32[4,1,576]{2,0,1:T(4,128)}, u32[]{:S(2)}) copy-start(f32[4,1,576]{2,0,1:T(4,128)} %slice_bitcast_fusion.39) | copy-start | bytes 27652
  159.4 16.8 %copy-start.39 = (f32[4,1,576]{2,0,1:T(4,128)S(1)}, f32[4,1,576]{2,0,1:T(4,128)}, u32[]{:S(2)}) copy-start(f32[4,1,576]{2,0,1:T(4,128)} %slice_bitcast_fusion.38) | copy-start | bytes 27652
  159.4 16.8 %copy-start.40 = (f32[4,1,576]{2,0,1:T(4,128)S(1)}, f32[4,1,576]{2,0,1:T(4,128)}, u32[]{:S(2)}) copy-start(f32[4,1,576]{2,0,1:T(4,128)} %slice_bitcast_fusion.37) | copy-start | bytes 27652
  159.4 16.8 %copy-start.41 = (f32[4,1,576]{2,0,1:T(4,128)S(1)}, f32[4,1,576]{2,0,1:T(4,128)}, u32[]{:S(2)}) copy-start(f32[4,1,576]{2,0,1:T(4,128)} %slice_bitcast_fusion.36) | copy-start | bytes 27652
  159.4 21.9 %copy-start.6 = (f32[4,576]{1,0:T(4,128)S(1)}, f32[4,576]{1,0:T(4,128)}, u32[]{:S(2)}) copy-start(f32[4,576]{1,0:T(4,128)} %get-tuple-element.64) | copy-start | bytes 27652
  159.4 22.7 %copy-start.5 = (f32[4,576]{1,0:T(4,128)S(1)}, f32[4,576]{1,0:T(4,128)}, u32[]{:S(2)}) copy-start(f32[4,576]{1,0:T(4,128)} %get-tuple-element.65) | copy-start | bytes 27652
  161.3 22.8 %copy-start.1 = (f32[256,512]{1,0:T(8,128)}, f32[256,512]{1,0:T(8,128)S(1)}, u32[]{:S(2)}) copy-start(f32[256,512]{1,0:T(8,128)S(1)} %get-tuple-element.183) | copy-start | bytes 1572868
  161.3 22.3 %copy-start.4 = (f32[4,576]{1,0:T(4,128)S(1)}, f32[4,576]{1,0:T(4,128)}, u32[]{:S(2)}) copy-start(f32[4,576]{1,0:T(4,128)} %get-tuple-element.66) | copy-start | bytes 27652
  168.1 16.1 %copy-start.3 = (f32[4,576]{1,0:T(4,128)S(1)}, f32[4,576]{1,0:T(4,128)}, u32[]{:S(2)}) copy-start(f32[4,576]{1,0:T(4,128)} %get-tuple-element.67) | copy-start | bytes 27652
  168.2 14.3 %collective-permute-start.3 = (bf16[256,512]{1,0:T(8,128)(2,1)S(1)}, bf16[256,512]{1,0:T(8,128)(2,1)S(1)}, u32[]{:S(2)}, u32[]{:S(2)}) collective-permute-start(bf16[256,512]{1,0:T(8,128)(2,1)S(1)} %multiply_convert_fusion), channel_id=1, source_target_pairs={{0,4},{4,8},{8,12},{12,16},{16,20},{20,24},{24,28},{1,5},{5,9},{9,... | collective-permute-start | bytes 786440 | tf_op jit(solution)/shard_map/ppermute | solution.py:18
  171.7 10.9 %collective-permute-start.2 = (bf16[256,512]{1,0:T(8,128)(2,1)S(1)}, bf16[256,512]{1,0:T(8,128)(2,1)S(1)}, u32[]{:S(2)}, u32[]{:S(2)}) collective-permute-start(bf16[256,512]{1,0:T(8,128)(2,1)S(1)} %multiply_convert_fusion), channel_id=1, source_target_pairs={{0,8},{4,12},{8,16},{12,20},{16,24},{20,28},{1,9},{5,13},{9,17},{1... | collective-permute-start | bytes 786440 | tf_op jit(solution)/shard_map/ppermute | solution.py:18
  243.4 10.0 %copy-start.2 = (f32[256,512]{1,0:T(8,128)S(1)}, f32[256,512]{1,0:T(8,128)}, u32[]{:S(2)}) copy-start(f32[256,512]{1,0:T(8,128)} %copy-done.1) | copy-start | bytes 1572868
  (4 other events, 13.5 us)
Sparse Core Ops, SparseCore 0:
  88.9 27.0 all-gather.2
  183.7 28.5 all-gather.4
where the time goes:
time: 264 us; the launch traced here: 263 us
  local copies, waits for them, and re-layouts  155 us (59%)
  matrix products  31.4 us (12%)
  blocking collectives  29 us (11%)
  between operations  15.7 us (6%)
  starting transfers between devices  14.1 us (5%)
  waiting for transfers between devices  11.2 us (4%)
  other arithmetic  6.69 us (3%)
    unnamed x222, local copies, waits for them, and re-layouts  59.2 us
    another operation x256, local copies, waits for them, and re-layouts, bias_table(): return jnp.stack(slices, axis=1)  52.5 us
    concatenate x77, local copies, waits for them, and re-layouts, band_blocks(): jnp.concatenate([blocked[offset_seg:offset_seg + segments] for offset_seg...  37.9 us
    psum x2, blocking collectives, normalize(): lax.psum(jnp.sum(values_f * values_f, axis=-1, keepdims=True), 'tp')  15.2 us
    ppermute x4, starting transfers between devices, from_behind(): return lax.ppermute(shard, axis, pairs)  13.8 us
    all_gather x2, blocking collectives, per_device(): lax.all_gather(attended, 'tp', axis=1, tiled=True)  13.8 us
    all_gather x2, waiting for transfers between devices, project_rows(): piece = lax.all_gather(rows_local, 'tp', axis=1, tiled=True)  11.2 us
    sub x2, matrix products, attend(): exponent = jnp.exp(scores - maximum)  7.36 us
  transfers between devices with their start and end apart: 6, of which 1 were waited for; matrix products, arithmetic and copies ran while one was open for 44% of the time, Pallas kernels for 0%

commit v1 on v0

--- a/solution.py
+++ b/solution.py
@@ -115,7 +115,7 @@
         attended = attend(query_rows, key_ext, value_ext, position_bias, visible)
         out_mat = out_weight[layer_index]
         summed = residual.astype(jnp.float32) + jnp.dot(
-            lax.all_gather(attended, "tp", axis=1, tiled=True),
+            jnp.concatenate(lax.all_gather(attended, "tp"), axis=1),
             out_mat,
             preferred_element_type=jnp.float32,
         )

time: 264 us -> 264 us (level)
  no operation moved by 1% of the time
where the time goes in v1:
time: 264 us; the launch traced here: 263 us
  local copies, waits for them, and re-layouts  155 us (59%)
  matrix products  31.2 us (12%)
  blocking collectives  28.9 us (11%)
  between operations  15.8 us (6%)
  starting transfers between devices  14.1 us (5%)
  waiting for transfers between devices  11.2 us (4%)
  other arithmetic  6.69 us (3%)
    unnamed x222, local copies, waits for them, and re-layouts  59.2 us
    another operation x256, local copies, waits for them, and re-layouts, bias_table(): return jnp.stack(slices, axis=1)  52.5 us
    concatenate x77, local copies, waits for them, and re-layouts, band_blocks(): jnp.concatenate([blocked[offset_seg:offset_seg + segments] for offset_seg...  37.9 us
    psum x2, blocking collectives, normalize(): lax.psum(jnp.sum(values_f * values_f, axis=-1, keepdims=True), 'tp')  15.2 us
    ppermute x4, starting transfers between devices, from_behind(): return lax.ppermute(shard, axis, pairs)  13.8 us
    all_gather x2, blocking collectives, per_device(): lax.all_gather(attended, 'tp')  13.7 us
    all_gather x2, waiting for transfers between devices, project_rows(): piece = lax.all_gather(rows_local, 'tp', axis=1, tiled=True)  11.2 us
    sub x2, matrix products, attend(): exponent = jnp.exp(scores - maximum)  7.35 us
  transfers between devices with their start and end apart: 6, of which 1 were waited for; matrix products, arithmetic and copies ran while one was open for 44% of the time, Pallas kernels for 0%

profile of v1, /device:TPU:0, one launch (start us, length us, event | category | flops | bytes accessed | tf_op | source)
XLA Modules:
  0.0 262.8 jit_solution(10276899425010949764)
XLA Ops:
  6.5 1.1 fusion.49
  7.6 8.4 %psum.14 = f32[256,1]{0,1:T(1,128)S(1)} all-reduce(f32[256,1]{0,1:T(1,128)S(1)} %bitcast.570), channel_id=1, replica_groups=mesh['sp'=8,'tp'=4] {'tp'}, use_global_device_ids=true, to_apply=%region_1.0 | all-reduce | flops 256 | bytes 2048 | tf_op jit(solution)/shard_map/psum | solution.py:23
  16.8 1.1 fusion.51
  17.9 3.4 %collective-permute-start.1 = (bf16[256,512]{1,0:T(8,128)(2,1)S(1)}, bf16[256,512]{1,0:T(8,128)(2,1)S(1)}, u32[]{:S(2)}, u32[]{:S(2)}) collective-permute-start(bf16[256,512]{1,0:T(8,128)(2,1)S(1)} %fusion.51), channel_id=1, source_target_pairs={{0,4},{4,8},{8,12},{12,16},{16,20},{20,24},{24,28},{1,5},{5,9},{9,... | collective-permute-start | bytes 786440 | tf_op jit(solution)/shard_map/ppermute | solution.py:18
  21.3 3.5 %collective-permute-start = (bf16[256,512]{1,0:T(8,128)(2,1)S(1)}, bf16[256,512]{1,0:T(8,128)(2,1)S(1)}, u32[]{:S(2)}, u32[]{:S(2)}) collective-permute-start(bf16[256,512]{1,0:T(8,128)(2,1)S(1)} %fusion.51), channel_id=1, source_target_pairs={{0,8},{4,12},{8,16},{12,20},{16,24},{20,28},{1,9},{5,13},{9,17},{1... | collective-permute-start | bytes 786440 | tf_op jit(solution)/shard_map/ppermute | solution.py:18
  87.8 0.9 pad_maximum_fusion
  95.7 2.0 reverse.211
  98.3 6.1 %stack.454 = f32[4,64,576]{2,1,0:T(8,128)} concatenate(f32[4,1,576]{2,1,0:T(1,128)S(1)} %copy.363, f32[4,1,576]{2,1,0:T(1,128)S(1)} %copy.364, f32[4,1,576]{2,1,0:T(1,128)S(1)} %copy.365, f32[4,1,576]{2,1,0:T(1,128)S(1)} %copy.366, f32[4,1,576]{2,1,0:T(1,128)S(1)} %copy.367, f32[4,1,576]{2,1,0:T(1,128)S(1)} %copy.368, f32[4,1,576]{2,1,0:T(1,128)S(1)} %copy.369, ...), dimensions={1} | concatenate | bytes 1179648 | tf_op jit(solution)/shard_map/stack | solution.py:37
  118.5 2.1 convolution_convert_fusion.5
  121.5 2.2 convolution_convert_fusion.3
  127.8 3.1 %convolution_convert_fusion.2 = bf16[768,256]{1,0:T(8,128)(2,1)S(1)} fusion(bf16[768,2048]{1,0:T(8,128)(2,1)} %all-gather.3.cloned.1.call-done, bf16[2,2048,256]{2,1,0:T(8,128)(2,1)} %param.10), kind=kOutput, calls=%fused_computation.24 | convolution fusion | flops 805502976 | bytes 4587520 | tf_op jit(solution)/shard_map/dot_general | solution.py:45
  131.3 0.9 copy.361
  132.3 0.9 copy.360
  133.4 0.9 copy.359
  134.5 0.9 copy.358
  135.6 0.9 copy.357
  136.7 0.9 copy.356
  137.7 0.9 copy.355
  138.8 0.9 copy.354
  140.8 2.8 %concatenate.125 = bf16[4,576,4,64]{1,3,0,2:T(8,128)(2,1)S(1)} concatenate(bf16[4,64,4,64]{1,3,0,2:T(8,128)(2,1)} %copy.353, bf16[4,64,4,64]{1,3,0,2:T(8,128)(2,1)} %copy.354, bf16[4,64,4,64]{1,3,0,2:T(8,128)(2,1)} %copy.355, bf16[4,64,4,64]{1,3,0,2:T(8,128)(2,1)} %copy.356, bf16[4,64,4,64]{1,3,0,2:T(8,128)(2,1)} %copy.357, bf16[4,64,4,64]{1,3,0,2:T(8,128)(2,1)} %copy.358, ...), dimensions={1} | concatenate | bytes 2359296 | tf_op jit(solution)/shard_map/concatenate | solution.py:61
  143.6 3.7 %fusion.204 = (f32[4,4,64]{2,1,0:T(4,128)S(1)}, f32[4,4,64,576]{3,2,1,0:T(8,128)}) fusion(f32[4,64,576]{2,1,0:T(8,128)} %stack.454, pred[4,576]{1,0:T(4,128)(4,1)S(1)} %copy-done.42, bf16[4,576,4,64]{1,3,0,2:T(8,128)(2,1)S(1)} %concatenate.125, bf16[4,64,4,64]{3,2,1,0:T(4,128)(2,1)} %reshape.170), kind=kOutput, calls=%fused_computation.465 | convolution fusion | flops 78447168 | bytes 4266240 | tf_op jit(solution)/shard_map/sub | solution.py:84
  147.3 2.3 concatenate.114
  149.6 2.4 fusion.28
  152.4 6.5 %all_gather.13 = bf16[4,256,256]{2,1,0:T(8,128)(2,1)S(1)} all-gather(bf16[1,256,256]{2,1,0:T(8,128)(2,1)S(1)} %all_gather_reshape.6), channel_id=1, replica_groups=mesh['sp'=8,'tp'=4] {'tp'}, dimensions={0}, use_global_device_ids=true | all-gather | bytes 655360 | tf_op jit(solution)/shard_map/all_gather | solution.py:118
  159.5 1.8 multiply_reduce_fusion
  161.3 6.8 %psum.15 = f32[256,1]{0,1:T(1,128)S(1)} all-reduce(f32[256,1]{0,1:T(1,128)S(1)} %bitcast.571), channel_id=1, replica_groups=mesh['sp'=8,'tp'=4] {'tp'}, use_global_device_ids=true, to_apply=%region_5.6 | all-reduce | flops 256 | bytes 2048 | tf_op jit(solution)/shard_map/psum | solution.py:23
  168.3 3.4 %collective-permute-start.3 = (bf16[256,512]{1,0:T(8,128)(2,1)S(1)}, bf16[256,512]{1,0:T(8,128)(2,1)S(1)}, u32[]{:S(2)}, u32[]{:S(2)}) collective-permute-start(bf16[256,512]{1,0:T(8,128)(2,1)S(1)} %multiply_convert_fusion), channel_id=1, source_target_pairs={{0,4},{4,8},{8,12},{12,16},{16,20},{20,24},{24,28},{1,5},{5,9},{9,... | collective-permute-start | bytes 786440 | tf_op jit(solution)/shard_map/ppermute | solution.py:18
  171.7 3.5 %collective-permute-start.2 = (bf16[256,512]{1,0:T(8,128)(2,1)S(1)}, bf16[256,512]{1,0:T(8,128)(2,1)S(1)}, u32[]{:S(2)}, u32[]{:S(2)}) collective-permute-start(bf16[256,512]{1,0:T(8,128)(2,1)S(1)} %multiply_convert_fusion), channel_id=1, source_target_pairs={{0,8},{4,12},{8,16},{12,20},{16,24},{20,28},{1,9},{5,13},{9,17},{1... | collective-permute-start | bytes 786440 | tf_op jit(solution)/shard_map/ppermute | solution.py:18
  182.6 0.9 pad_maximum_fusion.1
  195.0 6.1 %stack.519 = f32[4,64,576]{2,1,0:T(8,128)} concatenate(f32[4,1,576]{2,1,0:T(1,128)S(1)} %copy.448, f32[4,1,576]{2,1,0:T(1,128)S(1)} %copy.449, f32[4,1,576]{2,1,0:T(1,128)S(1)} %copy.450, f32[4,1,576]{2,1,0:T(1,128)S(1)} %copy.451, f32[4,1,576]{2,1,0:T(1,128)S(1)} %copy.452, f32[4,1,576]{2,1,0:T(1,128)S(1)} %copy.453, f32[4,1,576]{2,1,0:T(1,128)S(1)} %copy.454, ...), dimensions={1} | concatenate | bytes 1179648 | tf_op jit(solution)/shard_map/stack | solution.py:37
  201.1 11.2 %all-gather.5.cloned.1.call-done = bf16[768,2048]{1,0:T(8,128)(2,1)} async-done(((bf16[768,512]{1,0:T(8,128)(2,1)}), bf16[768,2048]{1,0:T(8,128)(2,1)}) %all-gather.5.cloned.1.call-update) | async-done | bytes 3145744 | tf_op jit(solution)/shard_map/all_gather | solution.py:43
  212.3 2.1 convolution_convert_fusion.4
  215.3 2.2 convolution_convert_fusion.1
  221.6 3.2 %convolution_convert_fusion = bf16[768,256]{1,0:T(8,128)(2,1)S(1)} fusion(bf16[768,2048]{1,0:T(8,128)(2,1)} %all-gather.5.cloned.1.call-done, bf16[2,2048,256]{2,1,0:T(8,128)(2,1)} %param.10), kind=kOutput, calls=%fused_computation.22 | convolution fusion | flops 805502976 | bytes 4587520 | tf_op jit(solution)/shard_map/dot_general | solution.py:45
  225.1 0.9 copy.446
  226.1 0.9 copy.445
  227.2 0.9 copy.444
  228.3 0.9 copy.443
  229.4 0.9 copy.442
  230.5 0.9 copy.441
  231.5 0.9 copy.440
  232.6 0.9 copy.439
  234.6 2.8 %concatenate.147 = bf16[4,576,4,64]{1,3,0,2:T(8,128)(2,1)S(1)} concatenate(bf16[4,64,4,64]{1,3,0,2:T(8,128)(2,1)} %copy.438, bf16[4,64,4,64]{1,3,0,2:T(8,128)(2,1)} %copy.439, bf16[4,64,4,64]{1,3,0,2:T(8,128)(2,1)} %copy.440, bf16[4,64,4,64]{1,3,0,2:T(8,128)(2,1)} %copy.441, bf16[4,64,4,64]{1,3,0,2:T(8,128)(2,1)} %copy.442, bf16[4,64,4,64]{1,3,0,2:T(8,128)(2,1)} %copy.443, ...), dimensions={1} | concatenate | bytes 2359296 | tf_op jit(solution)/shard_map/concatenate | solution.py:61
  237.4 3.7 %fusion.207 = (f32[4,4,64]{2,1,0:T(4,128)S(1)}, f32[4,4,64,576]{3,2,1,0:T(8,128)}) fusion(f32[4,64,576]{2,1,0:T(8,128)} %stack.519, pred[4,576]{1,0:T(4,128)(4,1)S(1)} %copy-done.43, bf16[4,576,4,64]{1,3,0,2:T(8,128)(2,1)S(1)} %concatenate.147, bf16[4,64,4,64]{3,2,1,0:T(4,128)(2,1)} %reshape.173), kind=kOutput, calls=%fused_computation.466 | convolution fusion | flops 78447168 | bytes 4266240 | tf_op jit(solution)/shard_map/sub | solution.py:84
  241.1 2.3 concatenate.137
  243.4 2.4 fusion.25
  246.2 7.2 %all_gather.15 = bf16[4,256,256]{2,1,0:T(8,128)(2,1)S(1)} all-gather(bf16[1,256,256]{2,1,0:T(8,128)(2,1)S(1)} %all_gather_reshape.7), channel_id=1, replica_groups=mesh['sp'=8,'tp'=4] {'tp'}, dimensions={0}, use_global_device_ids=true | all-gather | bytes 655360 | tf_op jit(solution)/shard_map/all_gather | solution.py:118
  253.6 2.4 fusion.17
  (581 shorter events, 119.0 us)
Async XLA Ops:
  6.5 112.0 %all-gather.3.cloned.1.call-start = ((), (), s32[]{:S(2)}) async-start(), calls=%async_computation | async-start | bytes 3932160 | tf_op jit(solution)/shard_map/all_gather | solution.py:43
  17.9 70.0 %collective-permute-start.1 = (bf16[256,512]{1,0:T(8,128)(2,1)S(1)}, bf16[256,512]{1,0:T(8,128)(2,1)S(1)}, u32[]{:S(2)}, u32[]{:S(2)}) collective-permute-start(bf16[256,512]{1,0:T(8,128)(2,1)S(1)} %fusion.51), channel_id=1, source_target_pairs={{0,4},{4,8},{8,12},{12,16},{16,20},{20,24},{24,28},{1,5},{5,9},{9,... | collective-permute-start | bytes 786440 | tf_op jit(solution)/shard_map/ppermute | solution.py:18
  21.3 66.5 %collective-permute-start = (bf16[256,512]{1,0:T(8,128)(2,1)S(1)}, bf16[256,512]{1,0:T(8,128)(2,1)S(1)}, u32[]{:S(2)}, u32[]{:S(2)}) collective-permute-start(bf16[256,512]{1,0:T(8,128)(2,1)S(1)} %fusion.51), channel_id=1, source_target_pairs={{0,8},{4,12},{8,16},{12,20},{16,24},{20,28},{1,9},{5,13},{9,17},{1... | collective-permute-start | bytes 786440 | tf_op jit(solution)/shard_map/ppermute | solution.py:18
  88.8 123.5 %all-gather.5.cloned.1.call-start = ((), (), s32[]{:S(2)}) async-start(), calls=%async_computation.1 | async-start | bytes 3932160 | tf_op jit(solution)/shard_map/all_gather | solution.py:43
  152.0 7.3 %copy-start = (bf16[256,512]{1,0:T(8,128)(2,1)S(1)}, bf16[256,512]{1,0:T(8,128)(2,1)}, u32[]{:S(2)}) copy-start(bf16[256,512]{1,0:T(8,128)(2,1)} %param.7) | copy-start | bytes 786436
  159.1 16.1 %copy-start.27 = (f32[4,640]{1,0:T(4,128)S(1)}, f32[4,640]{1,0:T(4,128)}, u32[]{:S(2)}) copy-start(f32[4,640]{1,0:T(4,128)} %reverse.211) | copy-start | bytes 30724
  159.1 16.1 %copy-start.7 = (f32[4,1,576]{2,0,1:T(4,128)S(1)}, f32[4,1,576]{2,0,1:T(4,128)}, u32[]{:S(2)}) copy-start(f32[4,1,576]{2,0,1:T(4,128)} %slice_bitcast_fusion.8) | copy-start | bytes 27652
  159.2 16.2 %copy-start.8 = (f32[4,1,576]{2,0,1:T(4,128)S(1)}, f32[4,1,576]{2,0,1:T(4,128)}, u32[]{:S(2)}) copy-start(f32[4,1,576]{2,0,1:T(4,128)} %slice_bitcast_fusion.7) | copy-start | bytes 27652
  159.2 16.2 %copy-start.9 = (f32[4,1,576]{2,0,1:T(4,128)S(1)}, f32[4,1,576]{2,0,1:T(4,128)}, u32[]{:S(2)}) copy-start(f32[4,1,576]{2,0,1:T(4,128)} %slice_bitcast_fusion.16) | copy-start | bytes 27652
  159.2 16.2 %copy-start.10 = (f32[4,1,576]{2,0,1:T(4,128)S(1)}, f32[4,1,576]{2,0,1:T(4,128)}, u32[]{:S(2)}) copy-start(f32[4,1,576]{2,0,1:T(4,128)} %slice_bitcast_fusion.15) | copy-start | bytes 27652
  159.2 16.2 %copy-start.11 = (f32[4,1,576]{2,0,1:T(4,128)S(1)}, f32[4,1,576]{2,0,1:T(4,128)}, u32[]{:S(2)}) copy-start(f32[4,1,576]{2,0,1:T(4,128)} %slice_bitcast_fusion.14) | copy-start | bytes 27652
  159.2 16.2 %copy-start.12 = (f32[4,1,576]{2,0,1:T(4,128)S(1)}, f32[4,1,576]{2,0,1:T(4,128)}, u32[]{:S(2)}) copy-start(f32[4,1,576]{2,0,1:T(4,128)} %slice_bitcast_fusion.13) | copy-start | bytes 27652
  159.2 16.3 %copy-start.13 = (f32[4,1,576]{2,0,1:T(4,128)S(1)}, f32[4,1,576]{2,0,1:T(4,128)}, u32[]{:S(2)}) copy-start(f32[4,1,576]{2,0,1:T(4,128)} %slice_bitcast_fusion.12) | copy-start | bytes 27652
  159.2 16.3 %copy-start.14 = (f32[4,1,576]{2,0,1:T(4,128)S(1)}, f32[4,1,576]{2,0,1:T(4,128)}, u32[]{:S(2)}) copy-start(f32[4,1,576]{2,0,1:T(4,128)} %slice_bitcast_fusion.11) | copy-start | bytes 27652
  159.2 16.3 %copy-start.15 = (f32[4,1,576]{2,0,1:T(4,128)S(1)}, f32[4,1,576]{2,0,1:T(4,128)}, u32[]{:S(2)}) copy-start(f32[4,1,576]{2,0,1:T(4,128)} %slice_bitcast_fusion.10) | copy-start | bytes 27652
  159.2 16.3 %copy-start.16 = (f32[4,1,576]{2,0,1:T(4,128)S(1)}, f32[4,1,576]{2,0,1:T(4,128)}, u32[]{:S(2)}) copy-start(f32[4,1,576]{2,0,1:T(4,128)} %slice_bitcast_fusion.9) | copy-start | bytes 27652
  159.2 16.3 %copy-start.17 = (f32[4,1,576]{2,0,1:T(4,128)S(1)}, f32[4,1,576]{2,0,1:T(4,128)}, u32[]{:S(2)}) copy-start(f32[4,1,576]{2,0,1:T(4,128)} %slice_bitcast_fusion.6) | copy-start | bytes 27652
  159.3 16.4 %copy-start.18 = (f32[4,1,576]{2,0,1:T(4,128)S(1)}, f32[4,1,576]{2,0,1:T(4,128)}, u32[]{:S(2)}) copy-start(f32[4,1,576]{2,0,1:T(4,128)} %slice_bitcast_fusion.24) | copy-start | bytes 27652
  159.3 16.4 %copy-start.19 = (f32[4,1,576]{2,0,1:T(4,128)S(1)}, f32[4,1,576]{2,0,1:T(4,128)}, u32[]{:S(2)}) copy-start(f32[4,1,576]{2,0,1:T(4,128)} %slice_bitcast_fusion.23) | copy-start | bytes 27652
  159.3 16.4 %copy-start.20 = (f32[4,1,576]{2,0,1:T(4,128)S(1)}, f32[4,1,576]{2,0,1:T(4,128)}, u32[]{:S(2)}) copy-start(f32[4,1,576]{2,0,1:T(4,128)} %slice_bitcast_fusion.22) | copy-start | bytes 27652
  159.3 16.4 %copy-start.21 = (f32[4,1,576]{2,0,1:T(4,128)S(1)}, f32[4,1,576]{2,0,1:T(4,128)}, u32[]{:S(2)}) copy-start(f32[4,1,576]{2,0,1:T(4,128)} %slice_bitcast_fusion.21) | copy-start | bytes 27652
  159.3 16.4 %copy-start.22 = (f32[4,1,576]{2,0,1:T(4,128)S(1)}, f32[4,1,576]{2,0,1:T(4,128)}, u32[]{:S(2)}) copy-start(f32[4,1,576]{2,0,1:T(4,128)} %slice_bitcast_fusion.20) | copy-start | bytes 27652
  159.3 16.5 %copy-start.23 = (f32[4,1,576]{2,0,1:T(4,128)S(1)}, f32[4,1,576]{2,0,1:T(4,128)}, u32[]{:S(2)}) copy-start(f32[4,1,576]{2,0,1:T(4,128)} %slice_bitcast_fusion.19) | copy-start | bytes 27652
  159.3 16.5 %copy-start.24 = (f32[4,1,576]{2,0,1:T(4,128)S(1)}, f32[4,1,576]{2,0,1:T(4,128)}, u32[]{:S(2)}) copy-start(f32[4,1,576]{2,0,1:T(4,128)} %slice_bitcast_fusion.18) | copy-start | bytes 27652
  159.3 16.5 %copy-start.25 = (f32[4,1,576]{2,0,1:T(4,128)S(1)}, f32[4,1,576]{2,0,1:T(4,128)}, u32[]{:S(2)}) copy-start(f32[4,1,576]{2,0,1:T(4,128)} %slice_bitcast_fusion.17) | copy-start | bytes 27652
  159.3 16.5 %copy-start.26 = (f32[4,1,576]{2,0,1:T(4,128)S(1)}, f32[4,1,576]{2,0,1:T(4,128)}, u32[]{:S(2)}) copy-start(f32[4,1,576]{2,0,1:T(4,128)} %slice_bitcast_fusion.5) | copy-start | bytes 27652
  159.4 16.5 %copy-start.28 = (f32[4,1,576]{2,0,1:T(4,128)S(1)}, f32[4,1,576]{2,0,1:T(4,128)}, u32[]{:S(2)}) copy-start(f32[4,1,576]{2,0,1:T(4,128)} %slice_bitcast_fusion.32) | copy-start | bytes 27652
  159.4 16.5 %copy-start.29 = (f32[4,1,576]{2,0,1:T(4,128)S(1)}, f32[4,1,576]{2,0,1:T(4,128)}, u32[]{:S(2)}) copy-start(f32[4,1,576]{2,0,1:T(4,128)} %slice_bitcast_fusion.31) | copy-start | bytes 27652
  159.4 16.6 %copy-start.30 = (f32[4,1,576]{2,0,1:T(4,128)S(1)}, f32[4,1,576]{2,0,1:T(4,128)}, u32[]{:S(2)}) copy-start(f32[4,1,576]{2,0,1:T(4,128)} %slice_bitcast_fusion.30) | copy-start | bytes 27652
  159.4 16.6 %copy-start.31 = (f32[4,1,576]{2,0,1:T(4,128)S(1)}, f32[4,1,576]{2,0,1:T(4,128)}, u32[]{:S(2)}) copy-start(f32[4,1,576]{2,0,1:T(4,128)} %slice_bitcast_fusion.29) | copy-start | bytes 27652
  159.4 16.6 %copy-start.32 = (f32[4,1,576]{2,0,1:T(4,128)S(1)}, f32[4,1,576]{2,0,1:T(4,128)}, u32[]{:S(2)}) copy-start(f32[4,1,576]{2,0,1:T(4,128)} %slice_bitcast_fusion.28) | copy-start | bytes 27652
  159.4 16.6 %copy-start.33 = (f32[4,1,576]{2,0,1:T(4,128)S(1)}, f32[4,1,576]{2,0,1:T(4,128)}, u32[]{:S(2)}) copy-start(f32[4,1,576]{2,0,1:T(4,128)} %slice_bitcast_fusion.27) | copy-start | bytes 27652
  159.4 16.6 %copy-start.34 = (f32[4,1,576]{2,0,1:T(4,128)S(1)}, f32[4,1,576]{2,0,1:T(4,128)}, u32[]{:S(2)}) copy-start(f32[4,1,576]{2,0,1:T(4,128)} %slice_bitcast_fusion.26) | copy-start | bytes 27652
  159.4 16.7 %copy-start.35 = (f32[4,1,576]{2,0,1:T(4,128)S(1)}, f32[4,1,576]{2,0,1:T(4,128)}, u32[]{:S(2)}) copy-start(f32[4,1,576]{2,0,1:T(4,128)} %slice_bitcast_fusion.25) | copy-start | bytes 27652
  159.4 16.7 %copy-start.36 = (f32[4,1,576]{2,0,1:T(4,128)S(1)}, f32[4,1,576]{2,0,1:T(4,128)}, u32[]{:S(2)}) copy-start(f32[4,1,576]{2,0,1:T(4,128)} %slice_bitcast_fusion.4) | copy-start | bytes 27652
  159.4 16.7 %copy-start.37 = (f32[4,1,576]{2,0,1:T(4,128)S(1)}, f32[4,1,576]{2,0,1:T(4,128)}, u32[]{:S(2)}) copy-start(f32[4,1,576]{2,0,1:T(4,128)} %slice_bitcast_fusion.40) | copy-start | bytes 27652
  159.5 16.7 %copy-start.38 = (f32[4,1,576]{2,0,1:T(4,128)S(1)}, f32[4,1,576]{2,0,1:T(4,128)}, u32[]{:S(2)}) copy-start(f32[4,1,576]{2,0,1:T(4,128)} %slice_bitcast_fusion.39) | copy-start | bytes 27652
  159.5 16.7 %copy-start.39 = (f32[4,1,576]{2,0,1:T(4,128)S(1)}, f32[4,1,576]{2,0,1:T(4,128)}, u32[]{:S(2)}) copy-start(f32[4,1,576]{2,0,1:T(4,128)} %slice_bitcast_fusion.38) | copy-start | bytes 27652
  159.5 16.8 %copy-start.40 = (f32[4,1,576]{2,0,1:T(4,128)S(1)}, f32[4,1,576]{2,0,1:T(4,128)}, u32[]{:S(2)}) copy-start(f32[4,1,576]{2,0,1:T(4,128)} %slice_bitcast_fusion.37) | copy-start | bytes 27652
  159.5 16.8 %copy-start.41 = (f32[4,1,576]{2,0,1:T(4,128)S(1)}, f32[4,1,576]{2,0,1:T(4,128)}, u32[]{:S(2)}) copy-start(f32[4,1,576]{2,0,1:T(4,128)} %slice_bitcast_fusion.36) | copy-start | bytes 27652
  159.5 21.8 %copy-start.6 = (f32[4,576]{1,0:T(4,128)S(1)}, f32[4,576]{1,0:T(4,128)}, u32[]{:S(2)}) copy-start(f32[4,576]{1,0:T(4,128)} %get-tuple-element.64) | copy-start | bytes 27652
  159.5 22.6 %copy-start.5 = (f32[4,576]{1,0:T(4,128)S(1)}, f32[4,576]{1,0:T(4,128)}, u32[]{:S(2)}) copy-start(f32[4,576]{1,0:T(4,128)} %get-tuple-element.65) | copy-start | bytes 27652
  161.3 22.8 %copy-start.1 = (f32[256,512]{1,0:T(8,128)}, f32[256,512]{1,0:T(8,128)S(1)}, u32[]{:S(2)}) copy-start(f32[256,512]{1,0:T(8,128)S(1)} %get-tuple-element.183) | copy-start | bytes 1572868
  161.3 22.3 %copy-start.4 = (f32[4,576]{1,0:T(4,128)S(1)}, f32[4,576]{1,0:T(4,128)}, u32[]{:S(2)}) copy-start(f32[4,576]{1,0:T(4,128)} %get-tuple-element.66) | copy-start | bytes 27652
  168.2 16.1 %copy-start.3 = (f32[4,576]{1,0:T(4,128)S(1)}, f32[4,576]{1,0:T(4,128)}, u32[]{:S(2)}) copy-start(f32[4,576]{1,0:T(4,128)} %get-tuple-element.67) | copy-start | bytes 27652
  168.3 14.3 %collective-permute-start.3 = (bf16[256,512]{1,0:T(8,128)(2,1)S(1)}, bf16[256,512]{1,0:T(8,128)(2,1)S(1)}, u32[]{:S(2)}, u32[]{:S(2)}) collective-permute-start(bf16[256,512]{1,0:T(8,128)(2,1)S(1)} %multiply_convert_fusion), channel_id=1, source_target_pairs={{0,4},{4,8},{8,12},{12,16},{16,20},{20,24},{24,28},{1,5},{5,9},{9,... | collective-permute-start | bytes 786440 | tf_op jit(solution)/shard_map/ppermute | solution.py:18
  171.7 10.9 %collective-permute-start.2 = (bf16[256,512]{1,0:T(8,128)(2,1)S(1)}, bf16[256,512]{1,0:T(8,128)(2,1)S(1)}, u32[]{:S(2)}, u32[]{:S(2)}) collective-permute-start(bf16[256,512]{1,0:T(8,128)(2,1)S(1)} %multiply_convert_fusion), channel_id=1, source_target_pairs={{0,8},{4,12},{8,16},{12,20},{16,24},{20,28},{1,9},{5,13},{9,17},{1... | collective-permute-start | bytes 786440 | tf_op jit(solution)/shard_map/ppermute | solution.py:18
  245.8 7.8 %copy-start.2 = (f32[256,512]{1,0:T(8,128)S(1)}, f32[256,512]{1,0:T(8,128)}, u32[]{:S(2)}) copy-start(f32[256,512]{1,0:T(8,128)} %copy-done.1) | copy-start | bytes 1572868
  (4 other events, 13.5 us)
Sparse Core Ops, SparseCore 0:
  88.9 27.0 all-gather.2
  183.7 28.5 all-gather.4
